TPU v7x, 32 devices: a whole 2x2x4 slice. The times are simulated.
32 devices in a mesh: sp: 16 (over z, y, x), tp: 2 (over core).
Axes of the slice: x: 2, y: 2, z: 4, core: 2. Of those that a mesh axis runs over, the one named last changes fastest.
Arguments:
- queries: bfloat16 [2048, 1024], P('sp', 'tp'), may hold values from -5 to 5
- keys: bfloat16 [2048, 1024], P('sp', 'tp'), may hold values from -5 to 5
- values: bfloat16 [2048, 1024], P('sp', 'tp'), may hold values from -5 to 5
- in_gate: float32 [8, 2048], P('tp', 'sp'), may hold values from -7 to 213
- forget_gate: float32 [8, 2048], P('tp', 'sp'), may hold values from 0 to 17
- stream: bfloat16 [2048, 2048], P('sp', 'tp'), may hold values from -24 to 24
- head_gain: float32 [1024], replicated, may hold values from 0.1 to 1.9
- out_weight: bfloat16 [1024, 2048], P(None, 'tp'), may hold values from -0.1875 to 0.1875
- norm_gain: float32 [2048], replicated, may hold values from 0.1 to 1.9
- gate_weight: bfloat16 [2048, 5632], P('sp', 'tp'), may hold values from -0.125 to 0.125
- up_weight: bfloat16 [2048, 5632], P('sp', 'tp'), may hold values from -0.125 to 0.125
- down_weight: bfloat16 [2048, 5632], P('sp', 'tp'), may hold values from -0.15625 to 0.15625
Outputs:
- layer_out: float32 [2048, 2048], P('sp', 'tp')
All inputs are finite; a program needn't handle non-finite values.
Results may differ from a plain program's by a relative error of at most 0.004.
Values may be sent and summed in bfloat16 or wider, within the bound.
A program may use at most 128 MiB of HBM per device.

v0:
```python
import jax
import jax.numpy as jnp
from jax import lax
from jax.sharding import PartitionSpec as P

D = 2048
HEAD_DIM = 128
BLOCK = 128
norm_eps = 1e-06
far_below = -1e30


def entering_state(total):
    memory, top, fall = total
    devices, here = (lax.axis_size("sp"), lax.axis_index("sp"))
    heads, rows, columns = memory.shape
    own_tops = jnp.broadcast_to(jnp.stack([top, fall])[None], (devices, 2, heads))
    tops = lax.all_to_all(own_tops, "sp", 0, 0)
    all_top, all_fall = (tops[:, 0], tops[:, 1])
    index = jnp.arange(devices)
    between = (index[None, None, :] > jnp.arange(-1, devices)[None, :, None]) & (
        index[None, None, :] < index[:, None, None]
    )
    after = jnp.sum(jnp.where(between[..., None], all_fall[None, None], 0.0), axis=2)
    reach = jnp.concatenate([jnp.zeros((1, heads), jnp.float32), all_top])[None] + after
    earlier = jnp.arange(-1, devices)[None, :, None] < index[:, None, None]
    reach = jnp.where(earlier, reach, -jnp.inf)
    top_in = jnp.max(reach, axis=1)
    share = jnp.exp(reach - top_in[:, None])[:, 1:]
    pieces = lax.all_to_all(
        jnp.transpose(memory.reshape(heads, devices, rows // devices, columns), (1, 0, 2, 3)),
        "sp",
        0,
        0,
    )
    sums = jnp.einsum("kjh,jhde->khde", share, pieces, precision=lax.Precision.HIGHEST)
    back = lax.all_to_all(sums, "sp", 0, 0)
    memory_in = jnp.transpose(back, (1, 0, 2, 3)).reshape(heads, rows, columns)
    return (memory_in, lax.dynamic_index_in_dim(top_in, here, 0, False), jnp.zeros_like(fall))


def merge_states(earlier, later):
    memory_early, top_early, fall_early = earlier
    memory_late, top_late, fall_late = later
    new_top = jnp.maximum(fall_late + top_early, top_late)
    keep_early = jnp.exp(fall_late + top_early - new_top)
    keep_late = jnp.exp(top_late - new_top)
    memory = keep_early[..., None, None] * memory_early + keep_late[..., None, None] * memory_late
    return (memory, new_top, fall_early + fall_late)


def memory_cell(queries, keys, values, in_gate, forget_gate, own_gain):
    tokens = queries.shape[0]
    local_heads = in_gate.shape[0]
    blocks = tokens // BLOCK
    key_scale = HEAD_DIM ** (-0.5)
    query_blocks = queries.reshape(blocks, BLOCK, local_heads, HEAD_DIM)
    key_blocks = keys.reshape(blocks, BLOCK, local_heads, HEAD_DIM)
    value_blocks = values.reshape(blocks, BLOCK, local_heads, HEAD_DIM)
    gate_blocks = in_gate.reshape(local_heads, blocks, BLOCK)
    cumulative = jnp.cumsum(
        jax.nn.log_sigmoid(forget_gate).reshape(local_heads, blocks, BLOCK), axis=-1
    )
    block_fall = cumulative[..., -1]
    log_weight = block_fall[..., None] - cumulative + gate_blocks
    block_top = jnp.max(log_weight, axis=-1)
    key_weight = jnp.exp(log_weight - block_top[..., None]) * key_scale
    weighted = (jnp.transpose(key_weight, (1, 2, 0))[..., None] * key_blocks).astype(jnp.bfloat16)
    block_memory = jnp.einsum(
        "nshd,nshe->nhde", weighted, value_blocks, preferred_element_type=jnp.float32
    )
    neutral = (
        jnp.zeros((local_heads, HEAD_DIM, HEAD_DIM), jnp.float32),
        jnp.full((local_heads,), far_below, jnp.float32),
        jnp.zeros((local_heads,), jnp.float32),
    )

    def advance(running, summary):
        return (merge_states(running, summary), running)

    device_total, before_block = lax.scan(
        advance, neutral, (block_memory, block_top.T, block_fall.T)
    )
    entering = entering_state(device_total)
    memory_in, top_in, fall_in = merge_states(
        jax.tree.map(lambda member: member[None], entering), before_block
    )
    causal = lax.broadcasted_iota(jnp.int32, (BLOCK, BLOCK), 0) >= lax.broadcasted_iota(
        jnp.int32, (BLOCK, BLOCK), 1
    )
    spread = cumulative[..., :, None] - cumulative[..., None, :] + gate_blocks[..., None, :]
    spread = jnp.where(causal, spread, -jnp.inf)
    carried = cumulative + top_in.T[..., None]
    row_top = jnp.maximum(carried, jnp.max(spread, axis=-1))
    decay_weight = jnp.exp(spread - row_top[..., None])
    scores = jnp.einsum(
        "nthd,nshd->hnts", query_blocks, key_blocks, preferred_element_type=jnp.float32
    )
    weights = (scores * key_scale * decay_weight).astype(jnp.bfloat16)
    inner_part = jnp.einsum(
        "hnts,nshe->nthe", weights, value_blocks, preferred_element_type=jnp.float32
    )
    outer_part = jnp.einsum(
        "nthd,nhde->nthe",
        query_blocks.astype(jnp.float32),
        memory_in,
        precision=lax.Precision.HIGHEST,
    )
    readout = (
        jnp.transpose(jnp.exp(carried - row_top), (1, 2, 0))[..., None] * outer_part + inner_part
    )
    row_scale = lax.rsqrt(jnp.mean(readout * readout, axis=-1, keepdims=True) + norm_eps)
    head_scale = own_gain.reshape(local_heads, HEAD_DIM)
    normed_heads = (readout * row_scale * head_scale).astype(jnp.bfloat16)
    return normed_heads.reshape(tokens, local_heads * HEAD_DIM)


def local(
    queries,
    keys,
    values,
    in_gate,
    forget_gate,
    stream,
    head_gain,
    out_weight,
    norm_gain,
    gate_weight,
    up_weight,
    down_weight,
):
    column_index = lax.axis_index("tp")
    local_width = queries.shape[1]
    own_gain = lax.dynamic_slice_in_dim(head_gain, column_index * local_width, local_width)
    heads_out = memory_cell(queries, keys, values, in_gate, forget_gate, own_gain)
    columns = out_weight.shape[1]
    projected = jnp.dot(
        lax.all_gather(heads_out, "tp", axis=1, tiled=True),
        out_weight,
        preferred_element_type=jnp.float32,
    )
    mixed_stream = stream.astype(jnp.float32) + projected
    squares = lax.psum(jnp.sum(mixed_stream * mixed_stream, axis=1), "tp")
    factor = lax.rsqrt(squares / D + norm_eps)
    own_norm = lax.dynamic_slice_in_dim(norm_gain, column_index * columns, columns)
    own_normed = (mixed_stream * factor[:, None] * own_norm).astype(jnp.bfloat16)
    if 2 * own_normed.size * lax.axis_size("tp") < 3 * gate_weight.size:
        channel = move_tokens(own_normed, gate_weight, up_weight, down_weight)
    else:
        channel = move_weights(own_normed, gate_weight, up_weight, down_weight)
    return mixed_stream + 0.5 * channel


def move_tokens(own_normed, gate_weight, up_weight, down_weight):
    devices = lax.axis_size("sp")
    rows, units = gate_weight.shape
    own_units = units // devices
    weights = jnp.stack([gate_weight.T, up_weight.T, down_weight.T])
    weights = weights.reshape(3, devices, own_units, rows)
    weights = lax.all_to_all(weights, "sp", 1, 2)
    weights = weights.reshape(3, own_units, devices * rows)
    half = lax.all_gather(own_normed, "sp", axis=0, tiled=True)
    normed = lax.all_gather(half, "tp", axis=1, tiled=True)
    gate_acts = jnp.einsum("td,fd->tf", normed, weights[0], preferred_element_type=jnp.float32)
    up_acts = jnp.einsum("td,fd->tf", normed, weights[1], preferred_element_type=jnp.float32)
    hidden = (jax.nn.silu(gate_acts) * up_acts).astype(jnp.bfloat16)
    terms = jnp.einsum("tf,fd->td", hidden, weights[2], preferred_element_type=jnp.float32)
    terms = lax.psum_scatter(terms.astype(jnp.bfloat16), "tp", scatter_dimension=1, tiled=True)
    return lax.psum_scatter(terms, "sp", scatter_dimension=0, tiled=True).astype(jnp.float32)


def move_weights(own_normed, gate_weight, up_weight, down_weight):
    normed = lax.all_gather(own_normed, "tp", axis=1, tiled=True)
    gate_acts = jnp.dot(
        normed,
        lax.all_gather(gate_weight, "sp", axis=0, tiled=True),
        preferred_element_type=jnp.float32,
    )
    up_acts = jnp.dot(
        normed,
        lax.all_gather(up_weight, "sp", axis=0, tiled=True),
        preferred_element_type=jnp.float32,
    )
    hidden = (jax.nn.silu(gate_acts) * up_acts).astype(jnp.bfloat16)
    channel_terms = jnp.einsum(
        "df,tf->dt",
        lax.all_gather(down_weight, "sp", axis=0, tiled=True),
        hidden,
        preferred_element_type=jnp.float32,
    )
    channel = lax.psum_scatter(
        channel_terms.astype(jnp.bfloat16), "tp", scatter_dimension=0, tiled=True
    ).astype(jnp.float32)
    return channel.T


def solution(mesh):
    return jax.shard_map(
        local,
        mesh=mesh,
        in_specs=(
            P("sp", "tp"),
            P("sp", "tp"),
            P("sp", "tp"),
            P("tp", "sp"),
            P("tp", "sp"),
            P("sp", "tp"),
            P(),
            P(None, "tp"),
            P(),
            P("sp", "tp"),
            P("sp", "tp"),
            P("sp", "tp"),
        ),
        out_specs=P("sp", "tp"),
        check_vma=False,
    )
```

profile of v0, /device:TPU:0, one launch (start us, length us, event | category | flops | bytes accessed | tf_op | source)
XLA Modules:
  0.0 339.9 jit_solution(915699007568806377)
XLA Ops:
  6.5 0.9 fusion.53
  7.4 1.2 reduce_window_sum.13
  8.7 0.1 copy.154
  8.8 0.1 copy.127
  8.9 0.9 fusion.60
  9.8 0.1 copy.128
  9.9 0.1 copy.130
  10.0 0.6 broadcast_in_dim.92
  10.7 8.3 %all-to-all-start = ((f32[16,2,4]{2,1,0:T(2,128)}), f32[16,2,4]{2,1,0:T(2,128)S(1)}, u32[]{:S(2)}, u32[]{:S(2)}) async-start(f32[16,2,4]{2,1,0:T(2,128)} %broadcast_in_dim.92), calls=%async_computation | async-start | bytes 32768 | tf_op jit(solution)/shard_map/all_to_all | solution.py:18
  19.1 0.1 broadcast_and_fusion
  19.2 0.9 select_reduce_fusion.1
  20.1 1.0 copy.155
  21.2 1.0 copy.156
  22.2 4.1 %all-to-all-done = f32[16,2,4]{2,1,0:T(2,128)S(1)} async-done(((f32[16,2,4]{2,1,0:T(2,128)}), f32[16,2,4]{2,1,0:T(2,128)S(1)}, u32[]{:S(2)}, u32[]{:S(2)}) %all-to-all-start) | async-done | bytes 544 | tf_op jit(solution)/shard_map/all_to_all | solution.py:18
  26.6 0.2 select_reduce_fusion
  26.8 0.1 fusion.61
  26.9 0.2 fusion.48
  27.1 0.8 multiply_bitcast_fusion
  27.9 0.2 convolution_bitcast_fusion.3
  28.1 0.1 fusion.20
  28.2 11.9 %all_to_all.30 = f32[16,4,8,128]{3,2,1,0:T(8,128)S(1)} all-to-all(f32[16,4,8,128]{3,2,1,0:T(8,128)S(1)} %fusion.20), channel_id=1, replica_groups=mesh['sp'=16,'tp'=2] {'sp'}, dimensions={0} | all-to-all | bytes 524288 | tf_op jit(solution)/shard_map/all_to_all | solution.py:30
  40.1 0.5 convolution_bitcast_fusion.2
  40.6 0.8 copy.138
  41.4 3.5 %all-to-all-start.2 = ((f32[16,4,8,128]{3,2,1,0:T(8,128)}), f32[16,4,8,128]{3,2,1,0:T(8,128)S(1)}, u32[]{:S(2)}, u32[]{:S(2)}) async-start(f32[16,4,8,128]{3,2,1,0:T(8,128)} %copy.138), calls=%async_computation.2 | async-start | bytes 524288 | tf_op jit(solution)/shard_map/all_to_all | solution.py:37
  45.1 0.4 convolution_bitcast_fusion.1
  45.6 8.6 %all-to-all-done.2 = f32[16,4,8,128]{3,2,1,0:T(8,128)S(1)} async-done(((f32[16,4,8,128]{3,2,1,0:T(8,128)}), f32[16,4,8,128]{3,2,1,0:T(8,128)S(1)}, u32[]{:S(2)}, u32[]{:S(2)}) %all-to-all-start.2) | async-done | bytes 262176 | tf_op jit(solution)/shard_map/all_to_all | solution.py:37
  54.2 0.5 multiply_reduce_fusion.1
  54.7 0.1 multiply_convert_fusion.1
  54.8 2.0 all_gather.9
  56.8 0.5 multiply_reduce_fusion
  57.4 2.5 psum.7
  59.9 0.8 multiply_convert_fusion
  60.7 73.6 %all-gather.3.cloned.1.call-done = bf16[2048,1024]{1,0:T(8,128)(2,1)} async-done(((bf16[128,1024]{1,0:T(8,128)(2,1)}), bf16[2048,1024]{1,0:T(8,128)(2,1)}) %all-gather.3.cloned.1.call-update) | async-done | bytes 4194320 | tf_op jit(solution)/shard_map/all_gather | solution.py:162
  134.4 1.5 copy.145
  135.9 2.3 copy.146
  138.2 2.3 copy.147
  140.4 1.8 pad_maximum_fusion
  142.2 0.1 copy.148
  142.4 54.4 %all_to_all.31 = bf16[3,16,176,1,128]{4,2,3,0,1:T(8,128)(2,1)S(1)} all-to-all(bf16[3,16,176,1,128]{4,2,3,0,1:T(8,128)(2,1)S(1)} %copy.148), channel_id=1, replica_groups=mesh['sp'=16,'tp'=2] {'sp'}, dimensions={1} | all-to-all | bytes 4325376 | tf_op jit(solution)/shard_map/all_to_all | solution.py:160
  196.7 0.1 fusion.63
  196.9 0.2 copy.150
  197.1 1.1 copy.151
  198.2 1.1 copy.149
  199.2 7.6 %fusion.11 = f32[2048,176]{0,1:T(8,128)} fusion(bf16[2048,2048]{1,0:T(8,128)(2,1)} %all-gather.5.cloned.1.call-done, bf16[22,8,16,128]{3,2,1,0:T(8,128)(2,1)} %bitcast.129), kind=kOutput, calls=%fused_computation.18 | convolution fusion | flops 1476395008 | bytes 10551296 | tf_op jit(solution)/shard_map/td,fd->tf/dot_general | solution.py:164
  206.8 12.3 %convolution_convert_fusion = bf16[2048,2048]{1,0:T(8,128)(2,1)} fusion(bf16[2048,2048]{1,0:T(8,128)(2,1)} %all-gather.5.cloned.1.call-done, f32[2048,176]{0,1:T(8,128)} %fusion.11, bf16[22,8,16,128]{3,2,1,0:T(8,128)(2,1)} %bitcast.128, bf16[22,8,16,128]{3,2,1,0:T(8,128)(2,1)S(1)} %bitcast.127), kind=kOutput, calls=%fused_computation | convolution fusion | flops 2959147008 | bytes 19660800 | tf_op jit(solution)/shard_map/tf,fd->td/dot_general | solution.py:167
  219.2 13.6 %reduce-scatter.3.cloned.1.call-done = bf16[2048,1024]{1,0:T(8,128)(2,1)} async-done(((bf16[2048,2048]{1,0:T(8,128)(2,1)}), bf16[2048,1024]{1,0:T(8,128)(2,1)}) %reduce-scatter.3.cloned.1.call-update) | async-done | bytes 4194320 | tf_op jit(solution)/shard_map/reduce_scatter | solution.py:168
  232.9 98.7 %reduce-scatter.5.cloned.1.call-done = bf16[128,1024]{1,0:T(8,128)(2,1)} async-done(((bf16[2048,1024]{1,0:T(8,128)(2,1)}), bf16[128,1024]{1,0:T(8,128)(2,1)}) %reduce-scatter.5.cloned.1.call-update) | async-done | bytes 262160 | tf_op jit(solution)/shard_map/reduce_scatter | solution.py:169
  331.6 1.8 multiply_add_fusion
  (38 shorter events, 0.9 us)
Async XLA Ops:
  6.5 50.3 %copy-start = (bf16[1024,1024]{1,0:T(8,128)(2,1)S(1)}, bf16[1024,1024]{1,0:T(8,128)(2,1)}, u32[]{:S(2)}) copy-start(bf16[1024,1024]{1,0:T(8,128)(2,1)} %param.19) | copy-start | bytes 6291460
  6.5 38.6 %copy-start.3 = (f32[4,128]{1,0:T(4,128)S(1)}, f32[4,128]{1,0:T(4,128)}, u32[]{:S(2)}) copy-start(f32[4,128]{1,0:T(4,128)} %param.15) | copy-start | bytes 6148
  6.5 38.5 %copy-start.4 = (f32[1024]{0:T(1024)S(1)}, f32[1024]{0:T(1024)}, u32[]{:S(2)}) copy-start(f32[1024]{0:T(1024)} %param.18) | copy-start | bytes 12292
  6.5 38.6 %copy-start.2 = (bf16[128,512]{1,0:T(8,128)(2,1)S(1)}, bf16[128,512]{1,0:T(8,128)(2,1)}, u32[]{:S(2)}) copy-start(bf16[128,512]{1,0:T(8,128)(2,1)} %param.12) | copy-start | bytes 393220
  10.7 15.7 %all-to-all-start = ((f32[16,2,4]{2,1,0:T(2,128)}), f32[16,2,4]{2,1,0:T(2,128)S(1)}, u32[]{:S(2)}, u32[]{:S(2)}) async-start(f32[16,2,4]{2,1,0:T(2,128)} %broadcast_in_dim.92), calls=%async_computation | async-start | bytes 32768 | tf_op jit(solution)/shard_map/all_to_all | solution.py:18
  40.1 16.7 %copy-start.1 = (bf16[128,1024]{1,0:T(8,128)(2,1)S(1)}, bf16[128,1024]{1,0:T(8,128)(2,1)}, u32[]{:S(2)}) copy-start(bf16[128,1024]{1,0:T(8,128)(2,1)} %param.17) | copy-start | bytes 786436
  41.4 12.8 %all-to-all-start.2 = ((f32[16,4,8,128]{3,2,1,0:T(8,128)}), f32[16,4,8,128]{3,2,1,0:T(8,128)S(1)}, u32[]{:S(2)}, u32[]{:S(2)}) async-start(f32[16,4,8,128]{3,2,1,0:T(8,128)} %copy.138), calls=%async_computation.2 | async-start | bytes 524288 | tf_op jit(solution)/shard_map/all_to_all | solution.py:37
  45.0 89.4 %all-gather.3.cloned.1.call-start = ((), (), s32[]{:S(2)}) async-start(), calls=%async_computation.6 | async-start | bytes 4456448 | tf_op jit(solution)/shard_map/all_gather | solution.py:162
  54.7 5.2 %dynamic-slice-start = ((f32[2048]{0:T(1024)}, s32[]{:T(128)}), f32[1024]{0:T(1024)S(1)}, s32[]{:S(2)}) async-start(f32[2048]{0:T(1024)} %param.20, s32[]{:T(128)} %select_n.44), calls=%async_computation.10 | async-start | bytes 8704 | tf_op jit(solution)/shard_map/dynamic_slice | solution.py:145
  60.7 138.5 %all-gather.5.cloned.1.call-start = ((), (), s32[]{:S(2)}) async-start(), calls=%async_computation.7 | async-start | bytes 12582912 | tf_op jit(solution)/shard_map/all_gather | solution.py:163
  134.4 98.4 %reduce-scatter.3.cloned.1.call-start = ((), (), s32[]{:S(2)}) async-start(), calls=%async_computation.8 | async-start | bytes 12582912 | tf_op jit(solution)/shard_map/reduce_scatter | solution.py:168
  219.1 112.4 %reduce-scatter.5.cloned.1.call-start = ((), (), s32[]{:S(2)}) async-start(), calls=%async_computation.9 | async-start | bytes 4456448 | tf_op jit(solution)/shard_map/reduce_scatter | solution.py:169
Sparse Core Ops, SparseCore 0:
  60.8 73.5 all-gather.2
  135.9 18.4 all-gather.4
  219.3 13.5 reduce-scatter.2
  235.0 96.5 reduce-scatter.4
where the time goes:
time: 341 us; the launch traced here: 340 us
  waiting for transfers between devices  199 us (58%)
  blocking collectives  70.7 us (21%)
  matrix products  22 us (6%)
  between operations  13.3 us (4%)
  local copies, waits for them, and re-layouts  12.9 us (4%)
  starting transfers between devices  12.1 us (4%)
  other arithmetic  10.1 us (3%)
    reduce_scatter x1, waiting for transfers between devices, move_tokens(): lax.psum_scatter(terms, 'sp', scatter_dimension=0, tiled=True)  98.7 us
    all_gather x1, waiting for transfers between devices, move_tokens(): half = lax.all_gather(own_normed, 'sp', axis=0, tiled=True)  73.6 us
    all_to_all x1, blocking collectives, move_tokens(): weights = lax.all_to_all(weights, 'sp', 1, 2)  54.4 us
    reduce_scatter x1, waiting for transfers between devices, move_tokens(): lax.psum_scatter(terms.astype(jnp.bfloat16), 'tp', scatter_dimension=1, t...  13.6 us
    dot_general x1, matrix products, move_tokens(): jnp.einsum('tf,fd->td', hidden, weights[2], preferred_element_type=jnp.fl...  12.3 us
    all_to_all x1, blocking collectives, entering_state(): lax.all_to_all(jnp.transpose(memory.reshape(heads, devices, rows // devic...  11.9 us
    all_to_all x1, waiting for transfers between devices, entering_state(): back = lax.all_to_all(sums, 'sp', 0, 0)  8.61 us
    all_to_all x1, starting transfers between devices, entering_state(): tops = lax.all_to_all(own_tops, 'sp', 0, 0)  8.34 us
  transfers between devices with their start and end apart: 6, of which 5 were waited for; matrix products, arithmetic and copies ran while one was open for 4% of the time, Pallas kernels for 0%

commit v1 on v0

--- a/solution.py
+++ b/solution.py
@@ -8,6 +8,22 @@
 BLOCK = 128
 norm_eps = 1e-06
 far_below = -1e30
+
+
+def gather_around(x, axis, dim):
+    ways, here, lap = (lax.axis_size(axis), lax.axis_index(axis), x.shape[dim])
+    lengths = [n * ways if d == dim else n for d, n in enumerate(x.shape)]
+    full = lax.dynamic_update_slice_in_dim(jnp.zeros(lengths, x.dtype), x, here * lap, axis=dim)
+    going_up = going_down = x
+    for far in range(1, ways // 2 + 1):
+        going_up = lax.ppermute(going_up, axis, [(d, (d + 1) % ways) for d in range(ways)])
+        full = lax.dynamic_update_slice_in_dim(full, going_up, (here - far) % ways * lap, axis=dim)
+        if 2 * far < ways:
+            going_down = lax.ppermute(going_down, axis, [(d, (d - 1) % ways) for d in range(ways)])
+            full = lax.dynamic_update_slice_in_dim(
+                full, going_down, (here + far) % ways * lap, axis=dim
+            )
+    return full
 
 
 def entering_state(total):
@@ -159,7 +175,7 @@
     weights = weights.reshape(3, devices, own_units, rows)
     weights = lax.all_to_all(weights, "sp", 1, 2)
     weights = weights.reshape(3, own_units, devices * rows)
-    half = lax.all_gather(own_normed, "sp", axis=0, tiled=True)
+    half = gather_around(own_normed, "sp", 0)
     normed = lax.all_gather(half, "tp", axis=1, tiled=True)
     gate_acts = jnp.einsum("td,fd->tf", normed, weights[0], preferred_element_type=jnp.float32)
     up_acts = jnp.einsum("td,fd->tf", normed, weights[1], preferred_element_type=jnp.float32)

time: 341 us -> 375 us (1.100)
  starting transfers between devices: 12.1 us -> 73.2 us
  waiting for transfers between devices: 199 us -> 152 us
  local copies, waits for them, and re-layouts: 12.9 us -> 30.8 us
    all_gather x1 -> x0, waiting for transfers between devices: 73.6 us -> none  [move_tokens(): half = lax.all_gather(own_normed, 'sp', axis=0, tiled=True)]
    ppermute x0 -> x15, starting transfers between devices: none -> 61.2 us  [the longest x7 50.1 us: gather_around(): lax.ppermute(going_down, axis, [(d, (d - 1) % ways) for d in range(ways)])]
    ppermute x0 -> x15, waiting for transfers between devices: none -> 28.6 us  [the longest x8 20 us: gather_around(): lax.ppermute(going_up, axis, [(d, (d + 1) % ways) for d in range(ways)])]
    dynamic_update_slice x0 -> x15, local copies, waits for them, and re-layouts: none -> 14.6 us  [the longest x8 7.66 us: gather_around(): lax.dynamic_update_slice_in_dim(full, going_up, (here - far) % ways * lap...]
  transfers between devices with their start and end apart: 6 -> 20, of which waited for: 5 -> 13; matrix products, arithmetic and copies ran while one was open for 4% -> 8% of each run, Pallas kernels for 0% -> 0%
where the time goes in v1:
time: 375 us; the launch traced here: 374 us
  waiting for transfers between devices  152 us (41%)
  starting transfers between devices  73.2 us (20%)
  blocking collectives  69.4 us (19%)
  local copies, waits for them, and re-layouts  30.8 us (8%)
  matrix products  23.6 us (6%)
  between operations  13.3 us (4%)
  other arithmetic  11.3 us (3%)
    reduce_scatter x1, waiting for transfers between devices, move_tokens(): lax.psum_scatter(terms, 'sp', scatter_dimension=0, tiled=True)  98.9 us
    all_to_all x1, blocking collectives, move_tokens(): weights = lax.all_to_all(weights, 'sp', 1, 2)  53.1 us
    ppermute x7, starting transfers between devices, gather_around(): lax.ppermute(going_down, axis, [(d, (d - 1) % ways) for d in range(ways)])  50.1 us
    ppermute x8, waiting for transfers between devices, gather_around(): lax.ppermute(going_up, axis, [(d, (d + 1) % ways) for d in range(ways)])  20 us
    reduce_scatter x1, waiting for transfers between devices, move_tokens(): lax.psum_scatter(terms.astype(jnp.bfloat16), 'tp', scatter_dimension=1, t...  13.7 us
    dot_general x1, matrix products, move_tokens(): jnp.einsum('tf,fd->td', hidden, weights[2], preferred_element_type=jnp.fl...  12.4 us
    all_to_all x1, blocking collectives, entering_state(): lax.all_to_all(jnp.transpose(memory.reshape(heads, devices, rows // devic...  11.9 us
    ppermute x8, starting transfers between devices, gather_around(): lax.ppermute(going_up, axis, [(d, (d + 1) % ways) for d in range(ways)])  11.1 us
  transfers between devices with their start and end apart: 20, of which 13 were waited for; matrix products, arithmetic and copies ran while one was open for 8% of the time, Pallas kernels for 0%

profile of v1, /device:TPU:0, one launch (start us, length us, event | category | flops | bytes accessed | tf_op | source)
XLA Modules:
  0.0 374.1 jit_solution(8075566663603124749)
XLA Ops:
  7.4 1.2 reduce_window_sum.13
  10.6 8.3 %all-to-all-start = ((f32[16,2,4]{2,1,0:T(2,128)}), f32[16,2,4]{2,1,0:T(2,128)S(1)}, u32[]{:S(2)}, u32[]{:S(2)}) async-start(f32[16,2,4]{2,1,0:T(2,128)} %broadcast_in_dim.95), calls=%async_computation | async-start | bytes 32768 | tf_op jit(solution)/shard_map/all_to_all | solution.py:34
  21.2 1.0 copy.156
  22.2 4.1 %all-to-all-done = f32[16,2,4]{2,1,0:T(2,128)S(1)} async-done(((f32[16,2,4]{2,1,0:T(2,128)}), f32[16,2,4]{2,1,0:T(2,128)S(1)}, u32[]{:S(2)}, u32[]{:S(2)}) %all-to-all-start) | async-done | bytes 544 | tf_op jit(solution)/shard_map/all_to_all | solution.py:34
  27.7 1.3 multiply_bitcast_fusion
  29.3 11.9 %all_to_all.30 = f32[16,4,8,128]{3,2,1,0:T(8,128)S(1)} all-to-all(f32[16,4,8,128]{3,2,1,0:T(8,128)S(1)} %fusion.23), channel_id=1, replica_groups=mesh['sp'=16,'tp'=2] {'sp'}, dimensions={0} | all-to-all | bytes 524288 | tf_op jit(solution)/shard_map/all_to_all | solution.py:46
  42.5 3.5 all-to-all-start.2
  46.9 1.3 convolution_bitcast_fusion.1
  48.3 7.0 %all-to-all-done.2 = f32[16,4,8,128]{3,2,1,0:T(8,128)S(1)} async-done(((f32[16,4,8,128]{3,2,1,0:T(8,128)}), f32[16,4,8,128]{3,2,1,0:T(8,128)S(1)}, u32[]{:S(2)}, u32[]{:S(2)}) %all-to-all-start.2) | async-done | bytes 262176 | tf_op jit(solution)/shard_map/all_to_all | solution.py:53
  55.3 1.1 multiply_reduce_fusion.1
  56.6 2.0 all_gather.6
  59.2 2.5 psum.7
  61.6 2.5 broadcast_in_dim.107
  65.7 4.9 %collective-permute-start.1 = (bf16[128,1024]{1,0:T(8,128)(2,1)S(1)}, bf16[128,1024]{1,0:T(8,128)(2,1)S(1)}, u32[]{:S(2)}, u32[]{:S(2)}) collective-permute-start(bf16[128,1024]{1,0:T(8,128)(2,1)S(1)} %get-tuple-element.27), channel_id=1, source_target_pairs={{0,30},{2,0},{4,2},{6,4},{8,6},{10,8},{12,10},{14,12},{16,14},{18,... | collective-permute-start | bytes 786440 | tf_op jit(solution)/shard_map/ppermute | solution.py:22
  70.6 6.6 %collective-permute-done = bf16[128,1024]{1,0:T(8,128)(2,1)S(1)} collective-permute-done((bf16[128,1024]{1,0:T(8,128)(2,1)S(1)}, bf16[128,1024]{1,0:T(8,128)(2,1)S(1)}, u32[]{:S(2)}, u32[]{:S(2)}) %collective-permute-start) | collective-permute-done | bytes 262176 | tf_op jit(solution)/shard_map/ppermute | solution.py:19
  77.3 2.5 collective-permute-start.2
  79.7 7.4 %collective-permute-start.3 = (bf16[128,1024]{1,0:T(8,128)(2,1)S(1)}, bf16[128,1024]{1,0:T(8,128)(2,1)}, u32[]{:S(2)}, u32[]{:S(2)}) collective-permute-start(bf16[128,1024]{1,0:T(8,128)(2,1)S(1)} %collective-permute-done.1), channel_id=1, source_target_pairs={{0,30},{2,0},{4,2},{6,4},{8,6},{10,8},{12,10},{14,12},{16,14},{18,... | collective-permute-start | bytes 786440 | tf_op jit(solution)/shard_map/ppermute | solution.py:22
  87.2 3.2 collective-permute-done.2
  90.4 2.5 collective-permute-start.4
  92.9 6.8 %collective-permute-start.5 = (bf16[128,1024]{1,0:T(8,128)(2,1)}, bf16[128,1024]{1,0:T(8,128)(2,1)S(1)}, u32[]{:S(2)}, u32[]{:S(2)}) collective-permute-start(bf16[128,1024]{1,0:T(8,128)(2,1)} %collective-permute-done.3), channel_id=1, source_target_pairs={{0,30},{2,0},{4,2},{6,4},{8,6},{10,8},{12,10},{14,12},{16,14},{18,... | collective-permute-start | bytes 786440 | tf_op jit(solution)/shard_map/ppermute | solution.py:22
  99.7 3.2 collective-permute-done.4
  103.0 2.6 collective-permute-start.6
  105.6 1.7 constant_dynamic-update-slice_fusion.14
  107.2 5.8 %collective-permute-start.7 = (bf16[128,1024]{1,0:T(8,128)(2,1)S(1)}, bf16[128,1024]{1,0:T(8,128)(2,1)S(1)}, u32[]{:S(2)}, u32[]{:S(2)}) collective-permute-start(bf16[128,1024]{1,0:T(8,128)(2,1)S(1)} %collective-permute-done.5), channel_id=1, source_target_pairs={{0,30},{2,0},{4,2},{6,4},{8,6},{10,8},{12,10},{14,12},{16,14},{18,... | collective-permute-start | bytes 786440 | tf_op jit(solution)/shard_map/ppermute | solution.py:22
  113.0 1.7 constant_dynamic-update-slice_fusion.13
  114.7 1.1 collective-permute-done.6
  115.8 2.4 collective-permute-start.8
  118.9 1.7 constant_dynamic-update-slice_fusion.11
  120.6 7.5 %collective-permute-start.9 = (bf16[128,1024]{1,0:T(8,128)(2,1)S(1)}, bf16[128,1024]{1,0:T(8,128)(2,1)S(1)}, u32[]{:S(2)}, u32[]{:S(2)}) collective-permute-start(bf16[128,1024]{1,0:T(8,128)(2,1)S(1)} %collective-permute-done.7), channel_id=1, source_target_pairs={{0,30},{2,0},{4,2},{6,4},{8,6},{10,8},{12,10},{14,12},{16,14},{18,... | collective-permute-start | bytes 786440 | tf_op jit(solution)/shard_map/ppermute | solution.py:22
  128.1 1.7 constant_dynamic-update-slice_fusion.10
  131.6 2.2 collective-permute-done.9
  133.8 9.6 %collective-permute-start.11 = (bf16[128,1024]{1,0:T(8,128)(2,1)S(1)}, bf16[128,1024]{1,0:T(8,128)(2,1)S(1)}, u32[]{:S(2)}, u32[]{:S(2)}) collective-permute-start(bf16[128,1024]{1,0:T(8,128)(2,1)S(1)} %collective-permute-done.9), channel_id=1, source_target_pairs={{0,30},{2,0},{4,2},{6,4},{8,6},{10,8},{12,10},{14,12},{16,14},{18,... | collective-permute-start | bytes 786440 | tf_op jit(solution)/shard_map/ppermute | solution.py:22
  145.6 3.6 collective-permute-done.11
  149.2 8.1 %collective-permute-start.13 = (bf16[128,1024]{1,0:T(8,128)(2,1)S(1)}, bf16[128,1024]{1,0:T(8,128)(2,1)S(1)}, u32[]{:S(2)}, u32[]{:S(2)}) collective-permute-start(bf16[128,1024]{1,0:T(8,128)(2,1)S(1)} %collective-permute-done.11), channel_id=1, source_target_pairs={{0,30},{2,0},{4,2},{6,4},{8,6},{10,8},{12,10},{14,12},{16,14},{18,... | collective-permute-start | bytes 786440 | tf_op jit(solution)/shard_map/ppermute | solution.py:22
  159.5 2.7 collective-permute-done.13
  162.9 5.8 %collective-permute-done.14 = bf16[128,1024]{1,0:T(8,128)(2,1)S(1)} collective-permute-done((bf16[128,1024]{1,0:T(8,128)(2,1)S(1)}, bf16[128,1024]{1,0:T(8,128)(2,1)S(1)}, u32[]{:S(2)}, u32[]{:S(2)}) %collective-permute-start.14) | collective-permute-done | bytes 262176 | tf_op jit(solution)/shard_map/ppermute | solution.py:19
  169.5 1.5 copy.145
  171.0 2.2 copy.146
  173.2 2.4 copy.147
  175.6 1.8 pad_maximum_fusion
  177.6 53.1 %all_to_all.31 = bf16[3,16,176,1,128]{4,2,3,0,1:T(8,128)(2,1)S(1)} all-to-all(bf16[3,16,176,1,128]{4,2,3,0,1:T(8,128)(2,1)S(1)} %copy.148), channel_id=1, replica_groups=mesh['sp'=16,'tp'=2] {'sp'}, dimensions={1} | all-to-all | bytes 4325376 | tf_op jit(solution)/shard_map/all_to_all | solution.py:176
  231.0 1.1 copy.151
  232.1 1.1 copy.149
  233.2 7.6 %fusion.14 = f32[2048,176]{0,1:T(8,128)} fusion(bf16[2048,2048]{1,0:T(8,128)(2,1)} %all-gather.2.cloned.1.call-done, bf16[22,8,16,128]{3,2,1,0:T(8,128)(2,1)} %bitcast.132), kind=kOutput, calls=%fused_computation.18 | convolution fusion | flops 1476395008 | bytes 10551296 | tf_op jit(solution)/shard_map/td,fd->tf/dot_general | solution.py:180
  240.7 12.4 %convolution_convert_fusion = bf16[2048,2048]{1,0:T(8,128)(2,1)} fusion(f32[2048,176]{0,1:T(8,128)} %fusion.14, bf16[22,8,16,128]{3,2,1,0:T(8,128)(2,1)} %bitcast.131, bf16[2048,2048]{1,0:T(8,128)(2,1)} %all-gather.2.cloned.1.call-done, bf16[22,8,16,128]{3,2,1,0:T(8,128)(2,1)S(1)} %bitcast.130), kind=kOutput, calls=%fused_computation | convolution fusion | flops 2959147008 | bytes 19660800 | tf_op jit(solution)/shard_map/tf,fd->td/dot_general | solution.py:183
  253.2 13.7 %reduce-scatter.3.cloned.1.call-done = bf16[2048,1024]{1,0:T(8,128)(2,1)} async-done(((bf16[2048,2048]{1,0:T(8,128)(2,1)}), bf16[2048,1024]{1,0:T(8,128)(2,1)}) %reduce-scatter.3.cloned.1.call-update) | async-done | bytes 4194320 | tf_op jit(solution)/shard_map/reduce_scatter | solution.py:184
  266.9 98.9 %reduce-scatter.5.cloned.1.call-done = bf16[128,1024]{1,0:T(8,128)(2,1)} async-done(((bf16[2048,1024]{1,0:T(8,128)(2,1)}), bf16[128,1024]{1,0:T(8,128)(2,1)}) %reduce-scatter.5.cloned.1.call-update) | async-done | bytes 262160 | tf_op jit(solution)/shard_map/reduce_scatter | solution.py:185
  365.8 1.8 multiply_add_fusion
  (83 shorter events, 20.1 us)
Async XLA Ops:
  6.5 52.1 %copy-start = (bf16[1024,1024]{1,0:T(8,128)(2,1)S(1)}, bf16[1024,1024]{1,0:T(8,128)(2,1)}, u32[]{:S(2)}) copy-start(bf16[1024,1024]{1,0:T(8,128)(2,1)} %param.19) | copy-start | bytes 6291460
  6.5 48.8 %copy-start.4 = (bf16[128,512]{1,0:T(8,128)(2,1)S(1)}, bf16[128,512]{1,0:T(8,128)(2,1)}, u32[]{:S(2)}) copy-start(bf16[128,512]{1,0:T(8,128)(2,1)} %param.12) | copy-start | bytes 393220
  6.5 52.1 %copy-start.3 = (bf16[128,1024]{1,0:T(8,128)(2,1)S(1)}, bf16[128,1024]{1,0:T(8,128)(2,1)}, u32[]{:S(2)}) copy-start(bf16[128,1024]{1,0:T(8,128)(2,1)} %param.17) | copy-start | bytes 786436
  10.6 15.7 %all-to-all-start = ((f32[16,2,4]{2,1,0:T(2,128)}), f32[16,2,4]{2,1,0:T(2,128)S(1)}, u32[]{:S(2)}, u32[]{:S(2)}) async-start(f32[16,2,4]{2,1,0:T(2,128)} %broadcast_in_dim.95), calls=%async_computation | async-start | bytes 32768 | tf_op jit(solution)/shard_map/all_to_all | solution.py:34
  19.1 7.5 %copy-start.5 = (pred[128,128]{1,0:T(8,128)(4,1)}, pred[128,128]{1,0:T(8,128)(4,1)S(1)}, u32[]{:S(2)}) copy-start(pred[128,128]{1,0:T(8,128)(4,1)S(1)} %iota_compare_fusion) | copy-start | bytes 49156
  42.5 12.8 %all-to-all-start.2 = ((f32[16,4,8,128]{3,2,1,0:T(8,128)}), f32[16,4,8,128]{3,2,1,0:T(8,128)S(1)}, u32[]{:S(2)}, u32[]{:S(2)}) async-start(f32[16,4,8,128]{3,2,1,0:T(8,128)} %copy.138), calls=%async_computation.2 | async-start | bytes 524288 | tf_op jit(solution)/shard_map/all_to_all | solution.py:53
  46.1 187.1 %all-gather.2.cloned.1.call-start = ((), (), s32[]{:S(2)}) async-start(), calls=%async_computation.6 | async-start | bytes 12582912 | tf_op jit(solution)/shard_map/all_gather | solution.py:179
  56.4 7.7 %dynamic-slice-start = ((f32[2048]{0:T(1024)}, s32[]{:T(128)}), f32[1024]{0:T(1024)S(1)}, s32[]{:S(2)}) async-start(f32[2048]{0:T(1024)} %param.20, s32[]{:T(128)} %select_n.155), calls=%async_computation.9 | async-start | bytes 8704 | tf_op jit(solution)/shard_map/dynamic_slice | solution.py:161
  65.0 12.3 %collective-permute-start = (bf16[128,1024]{1,0:T(8,128)(2,1)S(1)}, bf16[128,1024]{1,0:T(8,128)(2,1)S(1)}, u32[]{:S(2)}, u32[]{:S(2)}) collective-permute-start(bf16[128,1024]{1,0:T(8,128)(2,1)S(1)} %get-tuple-element.27), channel_id=1, source_target_pairs={{0,2},{2,4},{4,6},{6,8},{8,10},{10,12},{12,14},{14,16},{16,18},{18... | collective-permute-start | bytes 786440 | tf_op jit(solution)/shard_map/ppermute | solution.py:19
  65.7 14.0 %collective-permute-start.1 = (bf16[128,1024]{1,0:T(8,128)(2,1)S(1)}, bf16[128,1024]{1,0:T(8,128)(2,1)S(1)}, u32[]{:S(2)}, u32[]{:S(2)}) collective-permute-start(bf16[128,1024]{1,0:T(8,128)(2,1)S(1)} %get-tuple-element.27), channel_id=1, source_target_pairs={{0,30},{2,0},{4,2},{6,4},{8,6},{10,8},{12,10},{14,12},{16,14},{18,... | collective-permute-start | bytes 786440 | tf_op jit(solution)/shard_map/ppermute | solution.py:22
  77.3 25.7 %copy-start.2 = (bf16[128,1024]{1,0:T(8,128)(2,1)}, bf16[128,1024]{1,0:T(8,128)(2,1)S(1)}, u32[]{:S(2)}) copy-start(bf16[128,1024]{1,0:T(8,128)(2,1)S(1)} %collective-permute-done) | copy-start | bytes 786436
  77.3 13.1 %collective-permute-start.2 = (bf16[128,1024]{1,0:T(8,128)(2,1)S(1)}, bf16[128,1024]{1,0:T(8,128)(2,1)S(1)}, u32[]{:S(2)}, u32[]{:S(2)}) collective-permute-start(bf16[128,1024]{1,0:T(8,128)(2,1)S(1)} %collective-permute-done), channel_id=1, source_target_pairs={{0,2},{2,4},{4,6},{6,8},{8,10},{10,12},{12,14},{14,16},{16,18},{18... | collective-permute-start | bytes 786440 | tf_op jit(solution)/shard_map/ppermute | solution.py:19
  79.7 23.2 %copy-start.1 = (bf16[128,1024]{1,0:T(8,128)(2,1)}, bf16[128,1024]{1,0:T(8,128)(2,1)S(1)}, u32[]{:S(2)}) copy-start(bf16[128,1024]{1,0:T(8,128)(2,1)S(1)} %collective-permute-done.1) | copy-start | bytes 786436
  79.7 13.2 %collective-permute-start.3 = (bf16[128,1024]{1,0:T(8,128)(2,1)S(1)}, bf16[128,1024]{1,0:T(8,128)(2,1)}, u32[]{:S(2)}, u32[]{:S(2)}) collective-permute-start(bf16[128,1024]{1,0:T(8,128)(2,1)S(1)} %collective-permute-done.1), channel_id=1, source_target_pairs={{0,30},{2,0},{4,2},{6,4},{8,6},{10,8},{12,10},{14,12},{16,14},{18,... | collective-permute-start | bytes 786440 | tf_op jit(solution)/shard_map/ppermute | solution.py:22
  90.4 12.6 %collective-permute-start.4 = (bf16[128,1024]{1,0:T(8,128)(2,1)S(1)}, bf16[128,1024]{1,0:T(8,128)(2,1)}, u32[]{:S(2)}, u32[]{:S(2)}) collective-permute-start(bf16[128,1024]{1,0:T(8,128)(2,1)S(1)} %collective-permute-done.2), channel_id=1, source_target_pairs={{0,2},{2,4},{4,6},{6,8},{8,10},{10,12},{12,14},{14,16},{16,18},{18... | collective-permute-start | bytes 786440 | tf_op jit(solution)/shard_map/ppermute | solution.py:19
  92.9 14.3 %collective-permute-start.5 = (bf16[128,1024]{1,0:T(8,128)(2,1)}, bf16[128,1024]{1,0:T(8,128)(2,1)S(1)}, u32[]{:S(2)}, u32[]{:S(2)}) collective-permute-start(bf16[128,1024]{1,0:T(8,128)(2,1)} %collective-permute-done.3), channel_id=1, source_target_pairs={{0,30},{2,0},{4,2},{6,4},{8,6},{10,8},{12,10},{14,12},{16,14},{18,... | collective-permute-start | bytes 786440 | tf_op jit(solution)/shard_map/ppermute | solution.py:22
  103.0 12.8 %collective-permute-start.6 = (bf16[128,1024]{1,0:T(8,128)(2,1)}, bf16[128,1024]{1,0:T(8,128)(2,1)S(1)}, u32[]{:S(2)}, u32[]{:S(2)}) collective-permute-start(bf16[128,1024]{1,0:T(8,128)(2,1)} %collective-permute-done.4), channel_id=1, source_target_pairs={{0,2},{2,4},{4,6},{6,8},{8,10},{10,12},{12,14},{14,16},{16,18},{18... | collective-permute-start | bytes 786440 | tf_op jit(solution)/shard_map/ppermute | solution.py:19
  107.2 13.3 %collective-permute-start.7 = (bf16[128,1024]{1,0:T(8,128)(2,1)S(1)}, bf16[128,1024]{1,0:T(8,128)(2,1)S(1)}, u32[]{:S(2)}, u32[]{:S(2)}) collective-permute-start(bf16[128,1024]{1,0:T(8,128)(2,1)S(1)} %collective-permute-done.5), channel_id=1, source_target_pairs={{0,30},{2,0},{4,2},{6,4},{8,6},{10,8},{12,10},{14,12},{16,14},{18,... | collective-permute-start | bytes 786440 | tf_op jit(solution)/shard_map/ppermute | solution.py:22
  115.8 14.0 %collective-permute-start.8 = (bf16[128,1024]{1,0:T(8,128)(2,1)S(1)}, bf16[128,1024]{1,0:T(8,128)(2,1)S(1)}, u32[]{:S(2)}, u32[]{:S(2)}) collective-permute-start(bf16[128,1024]{1,0:T(8,128)(2,1)S(1)} %collective-permute-done.6), channel_id=1, source_target_pairs={{0,2},{2,4},{4,6},{6,8},{8,10},{10,12},{12,14},{14,16},{16,18},{18... | collective-permute-start | bytes 786440 | tf_op jit(solution)/shard_map/ppermute | solution.py:19
  120.6 13.3 %collective-permute-start.9 = (bf16[128,1024]{1,0:T(8,128)(2,1)S(1)}, bf16[128,1024]{1,0:T(8,128)(2,1)S(1)}, u32[]{:S(2)}, u32[]{:S(2)}) collective-permute-start(bf16[128,1024]{1,0:T(8,128)(2,1)S(1)} %collective-permute-done.7), channel_id=1, source_target_pairs={{0,30},{2,0},{4,2},{6,4},{8,6},{10,8},{12,10},{14,12},{16,14},{18,... | collective-permute-start | bytes 786440 | tf_op jit(solution)/shard_map/ppermute | solution.py:22
  129.8 14.4 %collective-permute-start.10 = (bf16[128,1024]{1,0:T(8,128)(2,1)S(1)}, bf16[128,1024]{1,0:T(8,128)(2,1)S(1)}, u32[]{:S(2)}, u32[]{:S(2)}) collective-permute-start(bf16[128,1024]{1,0:T(8,128)(2,1)S(1)} %collective-permute-done.8), channel_id=1, source_target_pairs={{0,2},{2,4},{4,6},{6,8},{8,10},{10,12},{12,14},{14,16},{16,18},{18... | collective-permute-start | bytes 786440 | tf_op jit(solution)/shard_map/ppermute | solution.py:19
  133.8 15.4 %collective-permute-start.11 = (bf16[128,1024]{1,0:T(8,128)(2,1)S(1)}, bf16[128,1024]{1,0:T(8,128)(2,1)S(1)}, u32[]{:S(2)}, u32[]{:S(2)}) collective-permute-start(bf16[128,1024]{1,0:T(8,128)(2,1)S(1)} %collective-permute-done.9), channel_id=1, source_target_pairs={{0,30},{2,0},{4,2},{6,4},{8,6},{10,8},{12,10},{14,12},{16,14},{18,... | collective-permute-start | bytes 786440 | tf_op jit(solution)/shard_map/ppermute | solution.py:22
  144.2 13.9 %collective-permute-start.12 = (bf16[128,1024]{1,0:T(8,128)(2,1)S(1)}, bf16[128,1024]{1,0:T(8,128)(2,1)S(1)}, u32[]{:S(2)}, u32[]{:S(2)}) collective-permute-start(bf16[128,1024]{1,0:T(8,128)(2,1)S(1)} %collective-permute-done.10), channel_id=1, source_target_pairs={{0,2},{2,4},{4,6},{6,8},{8,10},{10,12},{12,14},{14,16},{16,18},{18... | collective-permute-start | bytes 786440 | tf_op jit(solution)/shard_map/ppermute | solution.py:19
  149.2 13.0 %collective-permute-start.13 = (bf16[128,1024]{1,0:T(8,128)(2,1)S(1)}, bf16[128,1024]{1,0:T(8,128)(2,1)S(1)}, u32[]{:S(2)}, u32[]{:S(2)}) collective-permute-start(bf16[128,1024]{1,0:T(8,128)(2,1)S(1)} %collective-permute-done.11), channel_id=1, source_target_pairs={{0,30},{2,0},{4,2},{6,4},{8,6},{10,8},{12,10},{14,12},{16,14},{18,... | collective-permute-start | bytes 786440 | tf_op jit(solution)/shard_map/ppermute | solution.py:22
  158.0 10.7 %collective-permute-start.14 = (bf16[128,1024]{1,0:T(8,128)(2,1)S(1)}, bf16[128,1024]{1,0:T(8,128)(2,1)S(1)}, u32[]{:S(2)}, u32[]{:S(2)}) collective-permute-start(bf16[128,1024]{1,0:T(8,128)(2,1)S(1)} %collective-permute-done.12), channel_id=1, source_target_pairs={{0,2},{2,4},{4,6},{6,8},{8,10},{10,12},{12,14},{14,16},{16,18},{18... | collective-permute-start | bytes 786440 | tf_op jit(solution)/shard_map/ppermute | solution.py:19
  169.5 97.4 %reduce-scatter.3.cloned.1.call-start = ((), (), s32[]{:S(2)}) async-start(), calls=%async_computation.7 | async-start | bytes 12582912 | tf_op jit(solution)/shard_map/reduce_scatter | solution.py:184
  253.1 112.7 %reduce-scatter.5.cloned.1.call-start = ((), (), s32[]{:S(2)}) async-start(), calls=%async_computation.8 | async-start | bytes 4456448 | tf_op jit(solution)/shard_map/reduce_scatter | solution.py:185
Sparse Core Ops, SparseCore 0:
  169.6 17.9 all-gather.1
  253.2 13.6 reduce-scatter.2
  269.2 96.5 reduce-scatter.4
